TPU v7x, 32 devices: a whole 2x2x4 slice. The times are simulated.
32 devices in a mesh: sp: 8 (over z, x), tp: 4 (over y, core).
Axes of the slice: x: 2, y: 2, z: 4, core: 2. Of those that a mesh axis runs over, the one named last changes fastest.
Arguments:
- tokens: bfloat16 [1024, 2048], P('sp', 'tp'), may hold values from -6 to 6
- input_norm_gain: float32 [2048], replicated, may hold values from 0.1 to 1.9
- delta_query_projection: bfloat16 [2048, 512], P('sp', 'tp'), may hold values from -0.125 to 0.125
- delta_key_projection: bfloat16 [2048, 512], P('sp', 'tp'), may hold values from -0.125 to 0.125
- delta_value_projection: bfloat16 [2048, 512], P('sp', 'tp'), may hold values from -0.125 to 0.125
- delta_gate_projection: bfloat16 [2048, 512], P('sp', 'tp'), may hold values from -0.125 to 0.125
- write_strength_weight: bfloat16 [2048, 8], replicated, may hold values from -0.125 to 0.125
- decay_projection: bfloat16 [2048, 8], replicated, may hold values from -0.125 to 0.125
- write_strength_bias: float32 [8], P('tp'), as said below
- decay_scale_per_head: float32 [8], P('tp'), may hold values from 0 to 1
- decay_offset_terms: float32 [1024, 8], P('sp', 'tp'), may hold values from -1 to 0
- delta_norm_gain: float32 [64], replicated, may hold values from 0.1 to 1.9
- delta_output_projection: bfloat16 [2048, 512], P('sp', 'tp'), may hold values from -0.25 to 0.25
- window_query_projection: bfloat16 [2048, 1024], P('sp', 'tp'), may hold values from -1 to 1
- window_key_projection: bfloat16 [2048, 256], P('sp', 'tp'), may hold values from -1 to 1
- window_value_projection: bfloat16 [2048, 256], P('sp', 'tp'), may hold values from -0.125 to 0.125
- window_sink_logits: float32 [16], P('tp'), may hold values from 1 to 6
- window_output_projection: bfloat16 [2048, 1024], P('sp', 'tp'), may hold values from -0.1875 to 0.1875
Outputs:
- mixed: bfloat16 [1024, 2048], P(('sp', 'tp'))
- log_totals: float32 [1024, 16], P('sp', 'tp')
Inputs may be any that keep to these rules, and one draw needn't show every extreme that they name: `write_strength_bias`: at least the logarithm of 4 / 1024.
All inputs are finite; a program needn't handle non-finite values.
Results may differ from a plain program's by a relative error of at most 0.023.
The roundings to bfloat16 on the way count: a program that leaves them out, or rounds other values in their place, can miss the bound.
Values may be sent and summed in bfloat16 or wider, within the bound.
A program may use at most 64 MiB of HBM per device.

v0:
```python
import jax
import jax.numpy as jnp
from jax import lax
from jax.sharding import PartitionSpec as P

WINDOW = 128
DELTA_BLOCK_SIZE = 64


epsilon = 1e-06
rope_base = 500000.0
highest = lax.Precision.HIGHEST


def entering_2(value, axis, join, neutral):
    count, mine = (lax.axis_size(axis), lax.axis_index(axis))
    pieces = lax.all_gather(value, axis)
    subtotal = jnp.full_like(value, 0) + jnp.asarray(neutral, value.dtype)

    def lap(position, subtotal):
        longer = join(subtotal, pieces[position])
        return jnp.where(position < mine, longer, subtotal)

    return lax.fori_loop(0, count - 1, lap, subtotal)


def from_behind(value, axis, steps):
    count = lax.axis_size(axis)
    leading, last = (max(0, -steps), min(count, count - steps))
    return lax.ppermute(value, axis, [(source, source + steps) for source in range(leading, last)])


def unit_rows(values):
    return values * lax.rsqrt(jnp.sum(values * values, axis=-1, keepdims=True) + epsilon)


def rotate(values, positions):
    head_size = values.shape[-1]
    half_size = head_size // 2
    frequency = rope_base ** (-(2.0 / head_size) * jnp.arange(half_size, dtype=jnp.float32))
    angles = positions.astype(jnp.float32)[:, None] * frequency[None, :]
    cosine = jnp.cos(angles)[:, None, :]
    sine_part = jnp.sin(angles)[:, None, :]
    first_half = values[..., :half_size]
    second_half = values[..., half_size:]
    return jnp.concatenate(
        [
            first_half * cosine - second_half * sine_part,
            second_half * cosine + first_half * sine_part,
        ],
        axis=-1,
    )


def compose(earlier, later):
    head_size = later.shape[-2]
    linear = later[..., :head_size]
    moved = jnp.einsum("...de,...ef->...df", linear, earlier, precision=highest)
    return moved + jnp.concatenate([jnp.zeros_like(linear), later[..., head_size:]], axis=-1)


def delta_rule_mixer(
    query_accumulator,
    key_accumulator,
    value_accumulator,
    gate_accumulator,
    rate_preactivation,
    write_strength_bias,
    decay_scale_per_head,
    decay_offset_terms,
    delta_norm_gain,
):
    total_rows = query_accumulator.shape[0]
    number_of_heads = write_strength_bias.shape[0]
    head_size = delta_norm_gain.shape[0]
    block_list = total_rows // DELTA_BLOCK_SIZE

    def heads_first(values):
        return values.reshape(block_list, DELTA_BLOCK_SIZE, number_of_heads, head_size).transpose(
            2, 0, 1, 3
        )

    queries = unit_rows(heads_first(jax.nn.silu(query_accumulator))) * head_size ** (-0.5)
    key_rows = unit_rows(heads_first(jax.nn.silu(key_accumulator)))
    values = heads_first(jax.nn.silu(value_accumulator))
    write_rate = jax.nn.sigmoid(
        rate_preactivation[:, :number_of_heads] + write_strength_bias
    ).T.reshape(number_of_heads, block_list, DELTA_BLOCK_SIZE)
    decay_logarithm = (
        decay_offset_terms
        - decay_scale_per_head * jax.nn.softplus(rate_preactivation[:, number_of_heads:])
    ).T.reshape(number_of_heads, block_list, DELTA_BLOCK_SIZE)
    cumulative = jnp.cumsum(decay_logarithm, axis=-1)
    offsets_in = lax.iota(jnp.int32, DELTA_BLOCK_SIZE)
    lower_mask = offsets_in[:, None] >= offsets_in[None, :]
    strict = offsets_in[:, None] > offsets_in[None, :]
    within = jnp.where(lower_mask, cumulative[..., :, None] - cumulative[..., None, :], 0.0)
    decay_matrix = jnp.where(lower_mask, jnp.exp(within), 0.0)
    keys_written = key_rows * write_rate[..., None]
    key_gram = (
        jnp.einsum("hncd,hnsd->hncs", keys_written, key_rows, precision=highest) * decay_matrix
    )
    system = jnp.eye(DELTA_BLOCK_SIZE, dtype=jnp.float32) + jnp.where(strict, key_gram, 0.0)
    right_side = jnp.concatenate(
        [values * write_rate[..., None], keys_written * jnp.exp(cumulative)[..., None]], axis=-1
    )
    solved = jax.scipy.linalg.solve_triangular(system, right_side, lower=True)
    update_values = solved[..., :head_size]
    update_keys = solved[..., head_size:]
    update_both = jnp.concatenate([jnp.zeros_like(update_values), update_values], axis=-1)
    scores = jnp.einsum("hncd,hnsd->hncs", queries, key_rows, precision=highest) * decay_matrix
    queries_decayed = queries * jnp.exp(cumulative)[..., None]
    last_gate = cumulative[..., -1]
    keys_decayed = key_rows * jnp.exp(last_gate[..., None] - cumulative)[..., None]

    def advance(memory, inputs):
        value_block, weight_block, score_block, query_block, key_block, gate_block = inputs
        corrected = value_block - jnp.einsum(
            "hcd,hde->hce", weight_block, memory, precision=highest
        )
        output = jnp.einsum("hcd,hde->hce", query_block, memory, precision=highest) + jnp.einsum(
            "hcs,hse->hce", score_block, corrected, precision=highest
        )
        memory = memory * jnp.exp(gate_block)[:, None, None] + jnp.einsum(
            "hcd,hce->hde", key_block, corrected, precision=highest
        )
        return (memory, output)

    eye_stack = jnp.broadcast_to(
        jnp.eye(head_size, dtype=jnp.float32), (number_of_heads, head_size, head_size)
    )
    identity = jnp.concatenate(
        [eye_stack, jnp.zeros((number_of_heads, head_size, head_size), jnp.float32)], axis=-1
    )
    inputs = tuple(
        (
            jnp.moveaxis(tensor, 1, 0)
            for tensor in (
                update_both,
                update_keys,
                scores,
                queries_decayed,
                keys_decayed,
                last_gate,
            )
        )
    )
    transfer, outputs = lax.scan(advance, identity, inputs)
    entering = entering_2(transfer, "sp", compose, identity)
    carried = entering[..., head_size:]
    outputs = (
        jnp.einsum("nhcd,hde->nhce", outputs[..., :head_size], carried, precision=highest)
        + outputs[..., head_size:]
    )
    outputs = outputs.transpose(0, 2, 1, 3).reshape(total_rows, number_of_heads, head_size)
    normalized = (
        outputs
        * lax.rsqrt(jnp.mean(outputs * outputs, axis=-1, keepdims=True) + epsilon)
        * delta_norm_gain
    )
    gated = normalized * jax.nn.silu(gate_accumulator).reshape(
        total_rows, number_of_heads, head_size
    )
    return gated.astype(jnp.bfloat16).reshape(total_rows, number_of_heads * head_size)


def window_mixer(
    query_accumulator, key_accumulator, value_accumulator, window_sink_logits, positions, row_offset
):
    total_rows = query_accumulator.shape[0]
    query_heads = window_sink_logits.shape[0]
    head_size = query_accumulator.shape[1] // query_heads
    key_heads = key_accumulator.shape[1] // head_size
    group_size = query_heads // key_heads
    block_list = total_rows // WINDOW
    queries = rotate(
        query_accumulator.reshape(total_rows, query_heads, head_size), positions
    ).astype(jnp.bfloat16)
    key_rows = rotate(key_accumulator.reshape(total_rows, key_heads, head_size), positions).astype(
        jnp.bfloat16
    )
    keys_values = jnp.concatenate(
        [
            key_rows.reshape(total_rows, key_heads * head_size),
            value_accumulator.astype(jnp.bfloat16),
        ],
        axis=1,
    )
    edge_rows = from_behind(keys_values, "sp", 1)
    extended = jnp.concatenate([edge_rows, keys_values], axis=0).reshape(
        block_list + 1, WINDOW, 2, key_heads, head_size
    )
    band_rows = jnp.concatenate([extended[:-1], extended[1:]], axis=1)
    query_blocks = queries.reshape(block_list, WINDOW, key_heads, group_size, head_size)
    scores = jnp.einsum(
        "nqhgd,nkhd->nhgqk", query_blocks, band_rows[:, :, 0], preferred_element_type=jnp.float32
    ) * head_size ** (-0.5)
    query_in = lax.iota(jnp.int32, WINDOW)[:, None]
    key_in = lax.iota(jnp.int32, 2 * WINDOW)[None, :]
    key_start = row_offset + (lax.iota(jnp.int32, block_list) - 1) * WINDOW
    visible = ((key_in <= query_in + WINDOW) & (key_in > query_in))[None] & (
        key_start[:, None, None] + key_in[None] >= 0
    )
    visible = visible[:, None, None]
    sink_rows = window_sink_logits.reshape(key_heads, group_size)[None, :, :, None]
    row_top = jnp.maximum(jnp.max(jnp.where(visible, scores, -jnp.inf), axis=-1), sink_rows)
    weights = jnp.where(visible, jnp.exp(scores - row_top[..., None]), 0.0)
    row_total = jnp.sum(weights, axis=-1) + jnp.exp(sink_rows - row_top)
    log_totals = (
        (row_top + jnp.log(row_total)).transpose(0, 3, 1, 2).reshape(total_rows, query_heads)
    )
    weights_low = (weights / row_total[..., None]).astype(jnp.bfloat16)
    mixed_rows = jnp.einsum(
        "nhgqk,nkhd->nqhgd", weights_low, band_rows[:, :, 1], preferred_element_type=jnp.float32
    )
    mixed_rows = mixed_rows.astype(jnp.bfloat16).reshape(total_rows, query_heads * head_size)
    return (mixed_rows, log_totals)


def shards(
    tokens,
    input_norm_gain,
    delta_query_projection,
    delta_key_projection,
    delta_value_projection,
    delta_gate_projection,
    write_strength_weight,
    decay_projection,
    write_strength_bias,
    decay_scale_per_head,
    decay_offset_terms,
    delta_norm_gain,
    delta_output_projection,
    window_query_projection,
    window_key_projection,
    window_value_projection,
    window_sink_logits,
    window_output_projection,
):
    whole = lax.all_gather(tokens, "tp", axis=1, tiled=True)
    total_rows = whole.shape[0]
    widened = whole.astype(jnp.float32)
    normed = (
        widened
        * lax.rsqrt(jnp.mean(widened * widened, axis=1, keepdims=True) + epsilon)
        * input_norm_gain
    ).astype(jnp.bfloat16)
    row_offset = lax.axis_index("sp") * total_rows
    positions = row_offset + lax.iota(jnp.int32, total_rows)
    number_of_heads = write_strength_bias.shape[0]
    first_head = lax.axis_index("tp") * number_of_heads
    rate_weight = jnp.concatenate(
        [
            lax.dynamic_slice_in_dim(write_strength_weight, first_head, number_of_heads, 1),
            lax.dynamic_slice_in_dim(decay_projection, first_head, number_of_heads, 1),
        ],
        axis=1,
    )
    rate_preactivation = jnp.dot(normed, rate_weight, preferred_element_type=jnp.float32)

    def apply_projection(weight):
        return jnp.dot(normed, weight, preferred_element_type=jnp.float32)

    gathered = (
        lax.all_gather(delta_query_projection, "sp", axis=0, tiled=True),
        lax.all_gather(delta_key_projection, "sp", axis=0, tiled=True),
        lax.all_gather(delta_value_projection, "sp", axis=0, tiled=True),
        lax.all_gather(delta_gate_projection, "sp", axis=0, tiled=True),
        lax.all_gather(window_query_projection, "sp", axis=0, tiled=True),
        lax.all_gather(window_key_projection, "sp", axis=0, tiled=True),
        lax.all_gather(window_value_projection, "sp", axis=0, tiled=True),
        lax.all_gather(delta_output_projection, "sp", axis=0, tiled=True),
        lax.all_gather(window_output_projection, "sp", axis=0, tiled=True),
    )
    delta_mixed_output = delta_rule_mixer(
        apply_projection(gathered[0]),
        apply_projection(gathered[1]),
        apply_projection(gathered[2]),
        apply_projection(gathered[3]),
        rate_preactivation,
        write_strength_bias,
        decay_scale_per_head,
        decay_offset_terms,
        delta_norm_gain,
    )
    window_mix, log_totals = window_mixer(
        apply_projection(gathered[4]),
        apply_projection(gathered[5]),
        apply_projection(gathered[6]),
        window_sink_logits,
        positions,
        row_offset,
    )
    delta_full = gathered[7]
    window_full = gathered[8]
    delta_term = lax.dot_general(
        delta_mixed_output, delta_full, (((1,), (1,)), ((), ())), preferred_element_type=jnp.float32
    )
    window_term = lax.dot_general(
        window_mix, window_full, (((1,), (1,)), ((), ())), preferred_element_type=jnp.float32
    )
    mixed = lax.psum_scatter(
        (delta_term + window_term).astype(jnp.bfloat16), "tp", scatter_dimension=0, tiled=True
    )
    return (mixed, log_totals)


def solution(mesh):
    placed = (
        P("sp", "tp"),
        P(),
        P("sp", "tp"),
        P("sp", "tp"),
        P("sp", "tp"),
        P("sp", "tp"),
        P(),
        P(),
        P("tp"),
        P("tp"),
        P("sp", "tp"),
        P(),
        P("sp", "tp"),
        P("sp", "tp"),
        P("sp", "tp"),
        P("sp", "tp"),
        P("tp"),
        P("sp", "tp"),
    )
    return jax.shard_map(
        shards,
        mesh=mesh,
        in_specs=placed,
        out_specs=(P(("sp", "tp"), None), P("sp", "tp")),
        check_vma=False,
    )
```

profile of v0, /device:TPU:25, one launch (start us, length us, event | category | flops | bytes accessed | tf_op | source)
XLA Modules:
  0.0 337.4 jit_solution(10590593512638362334)
XLA Ops:
  7.2 0.7 all-gather.4.cloned.1.call-update
  8.0 22.7 %all_gather.44 = bf16[2048,64]{0,1:T(8,128)(2,1)S(1)} all-gather(bf16[256,64]{0,1:T(8,128)(2,1)S(1)} %copy-done.6), channel_id=1, replica_groups=mesh['sp'=8,'tp'=4] {'sp'}, dimensions={0}, use_global_device_ids=true | all-gather | bytes 294912 | tf_op jit(solution)/shard_map/all_gather | solution.py:270
  30.7 25.2 %all_gather.45 = bf16[2048,64]{0,1:T(8,128)(2,1)S(1)} all-gather(bf16[256,64]{0,1:T(8,128)(2,1)S(1)} %copy-done.7), channel_id=1, replica_groups=mesh['sp'=8,'tp'=4] {'sp'}, dimensions={0}, use_global_device_ids=true | all-gather | bytes 294912 | tf_op jit(solution)/shard_map/all_gather | solution.py:271
  55.9 19.3 %all_gather.36 = bf16[128,2048]{1,0:T(8,128)(2,1)S(1)} all-gather(bf16[128,512]{1,0:T(8,128)(2,1)S(1)} %copy-done), channel_id=1, replica_groups=mesh['sp'=8,'tp'=4] {'tp'}, dimensions={1}, use_global_device_ids=true | all-gather | bytes 655360 | tf_op jit(solution)/shard_map/all_gather | solution.py:240
  76.9 5.9 %collective-permute-start = (bf16[128,128]{0,1:T(8,128)(2,1)S(1)}, bf16[128,128]{0,1:T(8,128)(2,1)S(1)}, u32[]{:S(2)}, u32[]{:S(2)}) collective-permute-start(bf16[128,128]{0,1:T(8,128)(2,1)S(1)} %pad_maximum_fusion.1), channel_id=1, source_target_pairs={{0,4},{4,8},{8,12},{12,16},{16,20},{20,24},{24,28},{1,5},{5,9},{9,... | collective-permute-start | bytes 98312 | tf_op jit(solution)/shard_map/ppermute | solution.py:30
  82.9 0.8 constant_dynamic-slice_fusion.1
  85.2 23.4 %all_gather.37 = bf16[2048,128]{1,0:T(8,128)(2,1)S(1)} all-gather(bf16[256,128]{1,0:T(8,128)(2,1)S(1)} %copy-done.1), channel_id=1, replica_groups=mesh['sp'=8,'tp'=4] {'sp'}, dimensions={0}, use_global_device_ids=true | all-gather | bytes 589824 | tf_op jit(solution)/shard_map/all_gather | solution.py:266
  110.0 25.8 %all_gather.38 = bf16[2048,128]{1,0:T(8,128)(2,1)S(1)} all-gather(bf16[256,128]{1,0:T(8,128)(2,1)S(1)} %copy-done.2), channel_id=1, replica_groups=mesh['sp'=8,'tp'=4] {'sp'}, dimensions={0}, use_global_device_ids=true | all-gather | bytes 589824 | tf_op jit(solution)/shard_map/all_gather | solution.py:267
  136.8 19.7 %custom-call.4 = f32[2,2,1,64,64]{3,4,2,1,0:T(8,128)S(1)} custom-call(f32[2,2,1,64,64]{4,3,2,1,0:T(8,128)S(1)} %fusion.27), custom_call_target="InvertDiagBlocksLowerTriangular" | custom-call | tf_op jit(solution)/shard_map/jit(_solve_triangular)/vmap(vmap())/triangular_solve | solution.py:107
  157.2 0.7 copy-done.3
  157.9 25.4 %all_gather.39 = bf16[2048,128]{1,0:T(8,128)(2,1)S(1)} all-gather(bf16[256,128]{1,0:T(8,128)(2,1)S(1)} %copy-done.3), channel_id=1, replica_groups=mesh['sp'=8,'tp'=4] {'sp'}, dimensions={0}, use_global_device_ids=true | all-gather | bytes 589824 | tf_op jit(solution)/shard_map/all_gather | solution.py:265
  184.5 1.7 while.25
  186.3 25.2 %all-gather = f32[16,64,128]{2,1,0:T(8,128)S(1)} all-gather(f32[2,64,128]{2,1,0:T(8,128)S(1)} %get-tuple-element.129), channel_id=2, replica_groups=mesh['sp'=8,'tp'=4] {'sp'}, dimensions={0}, use_global_device_ids=true | all-gather | bytes 589824 | tf_op jit(solution)/shard_map/all_gather | solution.py:17
  211.5 2.3 while.26
  214.0 0.5 multiply_reduce_fusion
  215.0 0.7 copy-done.4
  215.7 25.8 %all_gather.42 = bf16[2048,128]{1,0:T(8,128)(2,1)S(1)} all-gather(bf16[256,128]{1,0:T(8,128)(2,1)S(1)} %copy-done.4), channel_id=1, replica_groups=mesh['sp'=8,'tp'=4] {'sp'}, dimensions={0}, use_global_device_ids=true | all-gather | bytes 589824 | tf_op jit(solution)/shard_map/all_gather | solution.py:268
  241.7 25.8 %all_gather.43 = bf16[2048,128]{1,0:T(8,128)(2,1)S(1)} all-gather(bf16[256,128]{1,0:T(8,128)(2,1)S(1)} %copy-done.5), channel_id=1, replica_groups=mesh['sp'=8,'tp'=4] {'sp'}, dimensions={0}, use_global_device_ids=true | all-gather | bytes 589824 | tf_op jit(solution)/shard_map/all_gather | solution.py:272
  267.5 1.7 fusion.97
  269.5 0.6 copy-done.9
  270.7 1.7 fusion.98
  272.4 1.4 fusion.19
  273.8 0.7 fusion.81
  274.5 56.5 %reduce-scatter.2.cloned.1.call-done = bf16[32,2048]{1,0:T(8,128)(2,1)} async-done(((bf16[128,2048]{1,0:T(8,128)(2,1)}), bf16[32,2048]{1,0:T(8,128)(2,1)}) %reduce-scatter.2.cloned.1.call-update) | async-done | bytes 131088 | tf_op jit(solution)/shard_map/reduce_scatter | solution.py:302
  (140 shorter events, 12.7 us)
Async XLA Ops:
  7.2 0.8 copy-start.6
  7.2 260.3 %all-gather.4.cloned.1.call-start = ((), (), s32[]{:S(2)}) async-start(), calls=%async_computation.1 | async-start | bytes 1179648 | tf_op jit(solution)/shard_map/all_gather | solution.py:269
  7.9 262.8 %all-gather.6.cloned.1.call-start = ((), (), s32[]{:S(2)}) async-start(), calls=%async_computation.2 | async-start | bytes 1179648 | tf_op jit(solution)/shard_map/all_gather | solution.py:273
  8.0 22.7 %copy-start.7 = (bf16[256,64]{0,1:T(8,128)(2,1)S(1)}, bf16[256,64]{0,1:T(8,128)(2,1)}, u32[]{:S(2)}) copy-start(bf16[256,64]{0,1:T(8,128)(2,1)} %param.37) | copy-start | bytes 98308
  30.7 25.2 %copy-start = (bf16[128,512]{1,0:T(8,128)(2,1)S(1)}, bf16[128,512]{1,0:T(8,128)(2,1)}, u32[]{:S(2)}) copy-start(bf16[128,512]{1,0:T(8,128)(2,1)} %param.22) | copy-start | bytes 393220
  75.2 0.7 copy-start.8
  76.9 192.4 %collective-permute-start = (bf16[128,128]{0,1:T(8,128)(2,1)S(1)}, bf16[128,128]{0,1:T(8,128)(2,1)S(1)}, u32[]{:S(2)}, u32[]{:S(2)}) collective-permute-start(bf16[128,128]{0,1:T(8,128)(2,1)S(1)} %pad_maximum_fusion.1), channel_id=1, source_target_pairs={{0,4},{4,8},{8,12},{12,16},{16,20},{20,24},{24,28},{1,5},{5,9},{9,... | collective-permute-start | bytes 98312 | tf_op jit(solution)/shard_map/ppermute | solution.py:30
  82.8 248.1 %reduce-scatter.2.cloned.1.call-start = ((), (), s32[]{:S(2)}) async-start(), calls=%async_computation.3 | async-start | bytes 655360 | tf_op jit(solution)/shard_map/reduce_scatter | solution.py:302
  83.7 0.7 copy-start.10
  83.7 0.7 copy-start.11
  83.7 0.7 copy-start.12
  83.7 1.5 copy-start.1
  109.1 0.8 copy-start.2
  157.0 0.8 copy-start.3
  214.9 0.8 copy-start.4
  215.7 25.8 %copy-start.13 = (f32[64]{0:T(128)S(1)}, f32[64]{0:T(128)}, u32[]{:S(2)}) copy-start(f32[64]{0:T(128)} %param.33) | copy-start | bytes 772
  215.7 26.0 %copy-start.5 = (bf16[256,128]{1,0:T(8,128)(2,1)S(1)}, bf16[256,128]{1,0:T(8,128)(2,1)}, u32[]{:S(2)}) copy-start(bf16[256,128]{1,0:T(8,128)(2,1)} %param.34) | copy-start | bytes 196612
  269.5 0.7 copy-start.9
Sparse Core Ops, SparseCore 0:
  10.1 39.6 all-gather.3
  82.9 38.8 all-gather.5
  273.9 56.9 reduce-scatter.1
where the time goes:
time: 340 us; the launch traced here: 337 us
  blocking collectives  219 us (64%)
  waiting for transfers between devices  57.2 us (17%)
  other arithmetic  22.6 us (7%)
  between operations  14.2 us (4%)
  matrix products  11.7 us (3%)
  local copies, waits for them, and re-layouts  6.71 us (2%)
  starting transfers between devices  6 us (2%)
    reduce_scatter x1, waiting for transfers between devices, shards(): lax.psum_scatter((delta_term + window_term).astype(jnp.bfloat16), 'tp', s...  56.5 us
    all_gather x1, blocking collectives, shards(): lax.all_gather(delta_value_projection, 'sp', axis=0, tiled=True)  25.8 us
    all_gather x1, blocking collectives, shards(): lax.all_gather(delta_output_projection, 'sp', axis=0, tiled=True)  25.8 us
    all_gather x1, blocking collectives, shards(): lax.all_gather(delta_gate_projection, 'sp', axis=0, tiled=True)  25.8 us
    all_gather x1, blocking collectives, shards(): lax.all_gather(delta_query_projection, 'sp', axis=0, tiled=True)  25.4 us
    all_gather x1, blocking collectives, entering_2(): pieces = lax.all_gather(value, axis)  25.2 us
    all_gather x1, blocking collectives, shards(): lax.all_gather(window_value_projection, 'sp', axis=0, tiled=True)  25.2 us
    all_gather x1, blocking collectives, shards(): lax.all_gather(delta_key_projection, 'sp', axis=0, tiled=True)  23.4 us
  transfers between devices with their start and end apart: 4, of which 1 were waited for; matrix products, arithmetic and copies ran while one was open for 10% of the time, Pallas kernels for 0%

commit v1 on v0

v1 whole, which is shorter than its diff:
```python
import functools

import jax
import jax.numpy as jnp
from jax import lax
from jax.experimental import pallas as pl
from jax.experimental.pallas import tpu as pltpu
from jax.sharding import PartitionSpec as P

WINDOW = 128
epsilon = 1e-06
rope_base = 500000.0
highest = lax.Precision.HIGHEST
MESH = pl.DeviceIdType.MESH
f32 = jnp.float32
bf16 = jnp.bfloat16


def dot_nn(a, b, precision=highest):
    return lax.dot_general(a, b, (((1,), (0,)), ((), ())), precision=precision, preferred_element_type=f32)


def dot_nt(a, b, precision=highest):
    return lax.dot_general(a, b, (((1,), (1,)), ((), ())), precision=precision, preferred_element_type=f32)


def dot_tn(a, b, precision=highest):
    return lax.dot_general(a, b, (((0,), (0,)), ((), ())), precision=precision, preferred_element_type=f32)


def silu(u):
    return u / (1.0 + jnp.exp(-u))


def unit_rows(u):
    return u * lax.rsqrt(jnp.sum(u * u, axis=-1, keepdims=True) + epsilon)


def iota(shape, dim):
    return lax.broadcasted_iota(jnp.int32, shape, dim)


def layer_kernel(
    S, T, G,
    tok_ref, gain_ref, dq_ref, dk_ref, dv_ref, dz_ref, ww_ref, wd_ref, bias_ref, scale_ref, offs_ref,
    ngain_ref, do_ref, wq_ref, wk_ref, wv_ref, sink_ref, wo_ref,
    mixed_ref, logt_ref,
    tokbuf, normed, Wd, Ww, Wo, st, edge_own, edge_in, mix, part, partin, memory,
    local_sem, tok_send, tok_recv, w_send, w_recv, st_send, st_recv, edge_send, edge_recv, out_send, out_recv,
):
    me = lax.axis_index("sp")
    j = lax.axis_index("tp")
    Z = S // G
    z = me // G
    x = me % G
    R, F = tok_ref.shape
    rows = dq_ref.shape[0]
    dc = dq_ref.shape[1]
    qc = wq_ref.shape[1]
    kc = wk_ref.shape[1]
    H = bias_ref.shape[0]
    E = dc // H
    QH = sink_ref.shape[0]
    mine = pl.ds(pl.multiple_of(me * rows, rows), rows)

    def local(i, src, dst):
        return pltpu.make_async_copy(src, dst, local_sem.at[i])

    locals_ = [
        local(0, dq_ref, Wd.at[mine, pl.ds(0, dc)]),
        local(1, dk_ref, Wd.at[mine, pl.ds(dc, dc)]),
        local(2, dv_ref, Wd.at[mine, pl.ds(2 * dc, dc)]),
        local(3, dz_ref, Wd.at[mine, pl.ds(3 * dc, dc)]),
        local(4, wq_ref, Ww.at[mine, pl.ds(0, qc)]),
        local(5, do_ref, Wo.at[mine, pl.ds(0, dc)]),
        local(6, wo_ref, Wo.at[mine, pl.ds(dc, qc)]),
        local(7, tok_ref, tokbuf.at[j]),
    ]
    for c in locals_:
        c.start()
    Ww[mine, pl.ds(qc, 2 * kc)] = jnp.concatenate([wk_ref[...], wv_ref[...]], axis=1)

    barrier = pltpu.get_barrier_semaphore()

    def greet_sp(d, _):
        pl.semaphore_signal(barrier, inc=1, device_id={"sp": lax.rem(me + d, S)}, device_id_type=MESH)
        return 0

    lax.fori_loop(1, S, greet_sp, 0)
    for d in range(1, T):
        pl.semaphore_signal(barrier, inc=1, device_id={"tp": lax.rem(j + d, T)}, device_id_type=MESH)
    pl.semaphore_wait(barrier, S - 1 + T - 1)

    def tok_copy(d):
        return pltpu.make_async_remote_copy(
            src_ref=tok_ref, dst_ref=tokbuf.at[j], send_sem=tok_send.at[d], recv_sem=tok_recv.at[j],
            device_id={"tp": lax.rem(j + d, T)}, device_id_type=MESH)

    for d in range(1, T):
        tok_copy(d).start()

    bufs = (Wd, Ww, Wo)

    def slab(g, p):
        return bufs[g].at[pl.ds(pl.multiple_of(p * rows, rows), rows), :]

    def wcopy(g, p, way):
        target = (me + G, me - G, me - x + lax.rem(x + 1, G))[way]
        return pltpu.make_async_remote_copy(
            src_ref=slab(g, p), dst_ref=slab(g, p), send_sem=w_send.at[g, way, p // G], recv_sem=w_recv.at[g, p],
            device_id={"sp": target}, device_id_type=MESH)

    def wait_slab(g, p):
        wcopy(g, p, 2 if G > 1 else 0).wait_recv()

    def forward(g, p, up, down):
        if up:
            @pl.when(z + 1 < Z)
            def _():
                wcopy(g, p, 0).start()
        if down:
            @pl.when(z > 0)
            def _():
                wcopy(g, p, 1).start()
        if G > 1:
            wcopy(g, p, 2).start()

    def relay(g, t):
        @pl.when(z - t >= 0)
        def _():
            p = (z - t) * G + x
            wait_slab(g, p)
            forward(g, p, True, False)

        @pl.when(z + t < Z)
        def _():
            p = (z + t) * G + x
            wait_slab(g, p)
            forward(g, p, False, True)

    def relays(g, low, high):
        def one(t, _):
            relay(g, t)
            return 0
        lax.fori_loop(low, high, one, 0)

    def finish(g):
        if G > 1:
            def one(zz, _):
                wait_slab(g, zz * G + lax.rem(x + 1, G))
                return 0
            lax.fori_loop(0, Z, one, 0)

    def drain(g):
        def one(zz, _):
            p = zz * G + x

            @pl.when((zz <= z) & (z + 1 < Z))
            def _():
                wcopy(g, p, 0).wait_send()

            @pl.when((zz >= z) & (z > 0))
            def _():
                wcopy(g, p, 1).wait_send()

            if G > 1:
                wcopy(g, p, 2).wait_send()
            return 0
        lax.fori_loop(0, Z, one, 0)

    for i in range(4):
        locals_[i].wait()
    forward(0, me, True, True)
    locals_[4].wait()
    forward(1, me, True, True)
    for i in (5, 6):
        locals_[i].wait()
    forward(2, me, True, True)

    half = E // 2
    lane = iota((R, E), 1)
    pair = jnp.where(lane < half, lane, lane - half).astype(f32)
    frequency = jnp.exp(pair * (-(2.0 / E)) * jnp.log(jnp.full((R, E), rope_base, f32)))
    angle = (me * R + iota((R, E), 0)).astype(f32) * frequency
    cosine = jnp.cos(angle)
    sine = jnp.sin(angle)
    ei = iota((E, E), 0)
    ej = iota((E, E), 1)
    swap = jnp.where(ei == ej + half, -1.0, 0.0) + jnp.where(ej == ei + half, 1.0, 0.0)

    locals_[7].wait()
    for d in range(1, T):
        src = lax.rem(j + d, T)
        pltpu.make_async_remote_copy(
            src_ref=tok_ref, dst_ref=tokbuf.at[src], send_sem=tok_send.at[d], recv_sem=tok_recv.at[src],
            device_id={"tp": lax.rem(j + d, T)}, device_id_type=MESH).wait_recv()
    total = jnp.zeros((R, 1), f32)
    for t in range(T):
        u = tokbuf[t].astype(f32)
        total = total + jnp.sum(u * u, axis=1, keepdims=True)
    inverse = lax.rsqrt(total / (T * F) + epsilon)
    for t in range(T):
        normed[:, t * F:(t + 1) * F] = (
            tokbuf[t].astype(f32) * inverse * gain_ref[:, t * F:(t + 1) * F]).astype(bf16)
    pre_w = jnp.dot(normed[...], ww_ref[...], preferred_element_type=f32)
    pre_d = jnp.dot(normed[...], wd_ref[...], preferred_element_type=f32)
    all_heads = pre_w.shape[1]
    head_lane = iota((R, all_heads), 1)

    relays(0, 1, Z)
    finish(0)
    proj = jnp.dot(normed[...], Wd[...], preferred_element_type=f32)

    ri = iota((R, R), 0)
    rj = iota((R, R), 1)
    lower = ri >= rj
    strict = ri > rj
    tril = jnp.where(lower, 1.0, 0.0)
    levels = []
    size = 1
    while size < R:
        levels.append(strict & (ri // (2 * size) == rj // (2 * size)) & (ri // size != rj // size))
        size *= 2
    keep = []
    for h in range(H):
        def head(n):
            return proj[:, n * dc + h * E:n * dc + (h + 1) * E]
        q = unit_rows(silu(head(0))) * E ** (-0.5)
        k = unit_rows(silu(head(1)))
        v = silu(head(2))
        chosen = head_lane == j * H + h
        write = jnp.sum(jnp.where(chosen, pre_w, 0.0), axis=1, keepdims=True) + bias_ref[h]
        decay = jnp.sum(jnp.where(chosen, pre_d, 0.0), axis=1, keepdims=True)
        beta = 1.0 / (1.0 + jnp.exp(-write))
        soft = jnp.maximum(decay, 0.0) + jnp.log1p(jnp.exp(-jnp.abs(decay)))
        logd = offs_ref[:, h:h + 1] - scale_ref[h] * soft
        C = dot_nn(tril, jnp.broadcast_to(logd, (R, R)))
        Dm = jnp.where(lower, jnp.exp(jnp.where(lower, C - C.T, 0.0)), 0.0)
        N = dot_nt(k * beta, k) * Dm
        X = jnp.where(ri == rj, 1.0, 0.0) - jnp.where(levels[0], N, 0.0)
        for mask in levels[1:]:
            X = X - dot_nn(X, dot_nn(jnp.where(mask, N, 0.0), X))
        C64 = C[:, :E]
        ec = jnp.exp(C64)
        U = dot_nn(X, v * beta)
        W = dot_nn(X, k * beta * ec)
        last = C64[R - 1:R, :]
        kd = k * jnp.exp(last - C64)
        Pm = dot_nt(q, k) * Dm
        st[me, h, :, 0:E] = jnp.where(ei == ej, jnp.exp(last), 0.0) - dot_tn(kd, W)
        st[me, h, :, E:2 * E] = dot_tn(kd, U)
        keep.append((dot_nn(Pm, U), q * ec - dot_nn(Pm, W)))

    def st_copy(d, p):
        return pltpu.make_async_remote_copy(
            src_ref=st.at[p], dst_ref=st.at[p], send_sem=st_send.at[d], recv_sem=st_recv.at[p],
            device_id={"sp": lax.rem(me + d, S)}, device_id_type=MESH)

    relays(1, 1, Z)

    def st_start(d, _):
        st_copy(d, me).start()
        return 0
    lax.fori_loop(1, S - me, st_start, 0)
    finish(1)
    wproj = jnp.dot(normed[...], Ww[...], preferred_element_type=f32)

    def rope(u):
        return u * cosine + dot_nn(u, swap) * sine
    k_cur = rope(wproj[:, qc:qc + kc]).astype(bf16)
    v_cur = wproj[:, qc + kc:qc + 2 * kc].astype(bf16)
    edge_own[:, 0:kc] = k_cur
    edge_own[:, kc:2 * kc] = v_cur
    queries = [rope(wproj[:, h * E:(h + 1) * E]).astype(bf16) for h in range(QH)]

    def edge_copy():
        return pltpu.make_async_remote_copy(
            src_ref=edge_own, dst_ref=edge_in, send_sem=edge_send, recv_sem=edge_recv,
            device_id={"sp": lax.rem(me + 1, S)}, device_id_type=MESH)
    edge_copy().start()
    relays(2, 1, Z)
    edge_copy().wait_recv()
    k_prev = edge_in[:, 0:kc]
    v_prev = edge_in[:, kc:2 * kc]
    seen_prev = (rj > ri) & (me > 0)
    for h in range(QH):
        s_cur = jnp.where(lower, dot_nt(queries[h], k_cur, None) * E ** (-0.5), -jnp.inf)
        s_prev = jnp.where(seen_prev, dot_nt(queries[h], k_prev, None) * E ** (-0.5), -jnp.inf)
        sink = sink_ref[h]
        top = jnp.maximum(jnp.maximum(jnp.max(s_cur, axis=1, keepdims=True), jnp.max(s_prev, axis=1, keepdims=True)), sink)
        e_cur = jnp.exp(s_cur - top)
        e_prev = jnp.exp(s_prev - top)
        row_total = (jnp.sum(e_cur, axis=1, keepdims=True) + jnp.sum(e_prev, axis=1, keepdims=True)
                     + jnp.exp(sink - top))
        logt_ref[:, h:h + 1] = top + jnp.log(row_total)
        mixed_rows = (dot_nn((e_cur / row_total).astype(bf16), v_cur, None)
                      + dot_nn((e_prev / row_total).astype(bf16), v_prev, None))
        mix[:, dc + h * E:dc + (h + 1) * E] = mixed_rows.astype(bf16)

    def chain(p, carry):
        pltpu.make_async_remote_copy(
            src_ref=st.at[p], dst_ref=st.at[p], send_sem=st_send.at[0], recv_sem=st_recv.at[p],
            device_id={"sp": lax.rem(me + 1, S)}, device_id_type=MESH).wait_recv()
        for h in range(H):
            memory[h] = dot_nn(st[p, h, :, 0:E], memory[h]) + st[p, h, :, E:2 * E]
        return carry
    memory[...] = jnp.zeros(memory.shape, f32)
    lax.fori_loop(0, me, chain, 0)
    for h in range(H):
        o = keep[h][0] + dot_nn(keep[h][1], memory[h])
        o = o * lax.rsqrt(jnp.mean(o * o, axis=1, keepdims=True) + epsilon) * ngain_ref[...]
        gate = proj[:, 3 * dc + h * E:3 * dc + (h + 1) * E]
        mix[:, h * E:(h + 1) * E] = (o * silu(gate)).astype(bf16)

    finish(2)
    part[...] = dot_nt(mix[...], Wo[...], None).astype(bf16)
    r = R // T

    def out_copy(d, source):
        peer = lax.rem(j + d, T)
        return pltpu.make_async_remote_copy(
            src_ref=part.at[pl.ds(pl.multiple_of(peer * r, r), r), :], dst_ref=partin.at[source],
            send_sem=out_send.at[d], recv_sem=out_recv.at[source],
            device_id={"tp": peer}, device_id_type=MESH)
    for d in range(1, T):
        out_copy(d, j).start()
    partin[j] = part[pl.ds(pl.multiple_of(j * r, r), r), :]
    for d in range(1, T):
        out_copy(d, lax.rem(j + d, T)).wait_recv()
    acc = partin[0].astype(f32)
    for t in range(1, T):
        acc = acc + partin[t].astype(f32)
    mixed_ref[...] = acc.astype(bf16)

    for d in range(1, T):
        out_copy(d, j).wait_send()
        tok_copy(d).wait_send()
    edge_copy().wait_send()

    def st_done(d, _):
        st_copy(d, me).wait_send()
        return 0
    lax.fori_loop(1, S - me, st_done, 0)
    for g in range(3):
        drain(g)


def shards(S, T, tokens, gain, dq, dk, dv, dz, ww, wd, bias, scale, offs, ngain, do, wq, wk, wv, sink, wo):
    R, F = tokens.shape
    D = F * T
    dc = dq.shape[1]
    H = bias.shape[0]
    E = dc // H
    qc, kc = wq.shape[1], wk.shape[1]
    G = 2 if S % 2 == 0 else 1
    Z = S // G
    vmem = pl.BlockSpec(memory_space=pltpu.VMEM)
    smem = pl.BlockSpec(memory_space=pltpu.SMEM)
    hbm = pl.BlockSpec(memory_space=pl.ANY)
    dma = pltpu.SemaphoreType.DMA
    return pl.pallas_call(
        functools.partial(layer_kernel, S, T, G),
        out_shape=(jax.ShapeDtypeStruct((R // T, D), bf16), jax.ShapeDtypeStruct((R, sink.shape[0]), f32)),
        in_specs=[vmem, vmem, hbm, hbm, hbm, hbm, vmem, vmem, smem, smem, vmem, vmem, hbm, hbm, vmem, vmem, smem, hbm],
        out_specs=(vmem, vmem),
        scratch_shapes=[
            pltpu.VMEM((T, R, F), bf16),
            pltpu.VMEM((R, D), bf16),
            pltpu.VMEM((D, 4 * dc), bf16),
            pltpu.VMEM((D, qc + 2 * kc), bf16),
            pltpu.VMEM((D, dc + qc), bf16),
            pltpu.VMEM((S, H, E, 2 * E), f32),
            pltpu.VMEM((R, 2 * kc), bf16),
            pltpu.VMEM((R, 2 * kc), bf16),
            pltpu.VMEM((R, dc + qc), bf16),
            pltpu.VMEM((R, D), bf16),
            pltpu.VMEM((T, R // T, D), bf16),
            pltpu.VMEM((H, E, E), f32),
            dma((8,)), dma((T,)), dma((T,)), dma((3, 3, Z)), dma((3, S)), dma((S,)), dma((S,)),
            dma, dma, dma((T,)), dma((T,)),
        ],
        compiler_params=pltpu.CompilerParams(
            collective_id=0, has_side_effects=True, vmem_limit_bytes=60 * 1024 * 1024),
    )(tokens, gain.reshape(1, D), dq, dk, dv, dz, ww, wd, bias, scale, offs, ngain.reshape(1, E), do, wq, wk, wv, sink, wo)


def solution(mesh):
    both = P("sp", "tp")
    placed = (both, P(), both, both, both, both, P(), P(), P("tp"), P("tp"), both, P(), both, both, both, both,
              P("tp"), both)
    return jax.shard_map(
        functools.partial(shards, mesh.shape["sp"], mesh.shape["tp"]),
        mesh=mesh, in_specs=placed, out_specs=(P(("sp", "tp"), None), both), check_vma=False)
```

time: 340 us -> 96.5 us (0.28)
  blocking collectives: 219 us -> 0 us
  Pallas kernels: 0 us -> 87.5 us
  waiting for transfers between devices: 57.2 us -> 0 us
  other arithmetic: 22.6 us -> 0 us
  between operations: 14.2 us -> 0.65 us
  matrix products: 11.7 us -> 0 us
  starting transfers between devices: 6 us -> 0 us
    all_gather x9 -> x0, blocking collectives: 219 us -> none  [the longest x1 25.8 us: shards(): lax.all_gather(delta_value_projection, 'sp', axis=0, tiled=True)]
    pallas_call x0 -> x1, Pallas kernels: none -> 87.5 us  [shards(): pl.pallas_call(functools.partial(layer_kernel, S, T, G), out_shape=(jax.S...]
    reduce_scatter x1 -> x0, waiting for transfers between devices: 56.5 us -> none  [shards(): lax.psum_scatter((delta_term + window_term).astype(jnp.bfloat16), 'tp', s...]
    another operation x4 -> x0, other arithmetic: 20.2 us -> none  [the longest x2 19.7 us: delta_rule_mixer(): solved = jax.scipy.linalg.solve_triangular(system, right_side, lower=True)]
    dot_general x29 -> x0, matrix products: 11.3 us -> none  [the longest x6 3.25 us: apply_projection(): return jnp.dot(normed, weight, preferred_element_type=jnp.float32)]
    ppermute x1 -> x0, starting transfers between devices: 5.88 us -> none  [from_behind(): lax.ppermute(value, axis, [(source, source + steps) for source in range(l...]
  transfers between devices with their start and end apart: 4 -> 0, of which waited for: 1 -> 0; matrix products, arithmetic and copies ran while one was open for 10% -> 0% of each run, Pallas kernels for 0% -> 0%
where the time goes in v1:
time: 96.5 us; the launch traced here: 96.1 us
  Pallas kernels  87.5 us (91%)
  local copies, waits for them, and re-layouts  8 us (8%)
    pallas_call x1, Pallas kernels, shards(): pl.pallas_call(functools.partial(layer_kernel, S, T, G), out_shape=(jax.S...  87.5 us
    unnamed x16, local copies, waits for them, and re-layouts  6.51 us

profile of v1, /device:TPU:25, one launch (start us, length us, event | category | flops | bytes accessed | tf_op | source)
XLA Modules:
  0.0 96.1 jit_solution(84395199221707443)
XLA Ops:
  0.6 0.0 copy-start.4
  0.6 0.7 copy-done.4
  1.3 0.0 copy-start
  1.3 0.7 copy.22.offs_ref
  2.1 0.0 copy-done
  2.1 0.0 copy-start.1
  2.1 0.7 copy.23.wk_ref
  2.8 0.0 copy-done.1
  2.8 0.0 copy-start.2
  2.8 0.7 copy.24.wv_ref
  3.5 0.0 copy-done.2
  3.6 0.0 copy-start.3
  3.6 1.0 %copy.20.ww_ref = bf16[2048,8]{1,0:T(8,128)(2,1)} copy(bf16[2048,8]{0,1:T(8,128)(2,1)S(1)} %copy-done.2) | data formatting | bytes 65536 | tf_op args[6]
  4.6 0.0 copy-done.3
  4.6 1.0 %copy.21.wd_ref = bf16[2048,8]{1,0:T(8,128)(2,1)} copy(bf16[2048,8]{0,1:T(8,128)(2,1)S(1)} %copy-done.3) | data formatting | bytes 65536 | tf_op args[7]
  5.6 87.5 %shard_map.185 = (bf16[32,2048]{1,0:T(8,128)(2,1)}, f32[128,4]{1,0:T(8,128)}) custom-call(bf16[128,512]{1,0:T(8,128)(2,1)} %tok_ref.1, f32[1,2048]{1,0:T(1,128)} %bitcast.2, bf16[256,128]{1,0:T(8,128)(2,1)} %dq_ref.1, bf16[256,128]{1,0:T(8,128)(2,1)} %dk_ref.1, bf16[256,128]{1,0:T(8,128)(2,1)} %dv_ref.1, bf16[256,128]{1,0:T(8,128)(2,1)} %dz_ref.1, ...), custom_call_target="tpu_custom_call" | custom-call | tf_op jit(solution)/shard_map/pallas_call | solution.py:361
  93.1 1.5 %copy.25 = f32[128,4]{0,1:T(4,128)} copy(f32[128,4]{1,0:T(8,128)} %get-tuple-element.3) | data formatting | bytes 4096 | tf_op jit(solution)/shard_map/pallas_call | solution.py:361
  94.5 1.6 %copy.27 = bf16[32,2048]{1,0:T(8,128)(2,1)} copy(bf16[32,2048]{1,0:T(8,128)(2,1)} %get-tuple-element.6) | data formatting | bytes 262144
Async XLA Ops:
  0.6 0.7 copy-start.4
  1.3 0.8 copy-start
  2.1 0.8 copy-start.1
  2.8 0.8 copy-start.2
  3.6 1.0 %copy-start.3 = (bf16[2048,8]{0,1:T(8,128)(2,1)S(1)}, bf16[2048,8]{0,1:T(8,128)(2,1)}, u32[]{:S(2)}) copy-start(bf16[2048,8]{0,1:T(8,128)(2,1)} %param.25) | copy-start | bytes 98308

commit v2 on v1

--- a/solution.py
+++ b/solution.py
@@ -45,23 +45,27 @@
     tok_ref, gain_ref, dq_ref, dk_ref, dv_ref, dz_ref, ww_ref, wd_ref, bias_ref, scale_ref, offs_ref,
     ngain_ref, do_ref, wq_ref, wk_ref, wv_ref, sink_ref, wo_ref,
     mixed_ref, logt_ref,
-    tokbuf, normed, Wd, Ww, Wo, st, edge_own, edge_in, mix, part, partin, memory,
+    tokbuf, feats, away, Wd, Ww, Wo, dpart, dpart_in, wpart, wpart_in, st, edge_own, edge_in, mix, part, partin,
+    red, red_in, memory,
     local_sem, tok_send, tok_recv, w_send, w_recv, st_send, st_recv, edge_send, edge_recv, out_send, out_recv,
+    pair_send, pair_recv,
 ):
     me = lax.axis_index("sp")
     j = lax.axis_index("tp")
     Z = S // G
     z = me // G
     x = me % G
+    other = lax.rem(x + 1, G)
     R, F = tok_ref.shape
     rows = dq_ref.shape[0]
+    K = Z * rows
     dc = dq_ref.shape[1]
     qc = wq_ref.shape[1]
-    kc = wk_ref.shape[1]
+    kc = wk_ref.shape[0]
     H = bias_ref.shape[0]
     E = dc // H
     QH = sink_ref.shape[0]
-    mine = pl.ds(pl.multiple_of(me * rows, rows), rows)
+    mine = pl.ds(pl.multiple_of(z * rows, rows), rows)
 
     def local(i, src, dst):
         return pltpu.make_async_copy(src, dst, local_sem.at[i])
@@ -78,7 +82,6 @@
     ]
     for c in locals_:
         c.start()
-    Ww[mine, pl.ds(qc, 2 * kc)] = jnp.concatenate([wk_ref[...], wv_ref[...]], axis=1)
 
     barrier = pltpu.get_barrier_semaphore()
 
@@ -89,6 +92,8 @@
     lax.fori_loop(1, S, greet_sp, 0)
     for d in range(1, T):
         pl.semaphore_signal(barrier, inc=1, device_id={"tp": lax.rem(j + d, T)}, device_id_type=MESH)
+    narrow = jnp.concatenate([wk_ref[...], wv_ref[...]], axis=0).astype(f32)
+    Ww[mine, pl.ds(qc, 2 * kc)] = narrow.T.astype(bf16)
     pl.semaphore_wait(barrier, S - 1 + T - 1)
 
     def tok_copy(d):
@@ -99,44 +104,41 @@
     for d in range(1, T):
         tok_copy(d).start()
 
+    def pair_copy(i, src, dst):
+        return pltpu.make_async_remote_copy(
+            src_ref=src, dst_ref=dst, send_sem=pair_send.at[i], recv_sem=pair_recv.at[i],
+            device_id={"sp": me - x + other}, device_id_type=MESH)
+
     bufs = (Wd, Ww, Wo)
 
-    def slab(g, p):
-        return bufs[g].at[pl.ds(pl.multiple_of(p * rows, rows), rows), :]
-
-    def wcopy(g, p, way):
-        target = (me + G, me - G, me - x + lax.rem(x + 1, G))[way]
-        return pltpu.make_async_remote_copy(
-            src_ref=slab(g, p), dst_ref=slab(g, p), send_sem=w_send.at[g, way, p // G], recv_sem=w_recv.at[g, p],
-            device_id={"sp": target}, device_id_type=MESH)
-
-    def wait_slab(g, p):
-        wcopy(g, p, 2 if G > 1 else 0).wait_recv()
-
-    def forward(g, p, up, down):
+    def slab(g, zz):
+        return bufs[g].at[pl.ds(pl.multiple_of(zz * rows, rows), rows), :]
+
+    def wcopy(g, zz, way):
+        return pltpu.make_async_remote_copy(
+            src_ref=slab(g, zz), dst_ref=slab(g, zz), send_sem=w_send.at[g, way, zz], recv_sem=w_recv.at[g, zz],
+            device_id={"sp": (me + G, me - G)[way]}, device_id_type=MESH)
+
+    def forward(g, zz, up, down):
         if up:
             @pl.when(z + 1 < Z)
             def _():
-                wcopy(g, p, 0).start()
+                wcopy(g, zz, 0).start()
         if down:
             @pl.when(z > 0)
             def _():
-                wcopy(g, p, 1).start()
-        if G > 1:
-            wcopy(g, p, 2).start()
+                wcopy(g, zz, 1).start()
 
     def relay(g, t):
         @pl.when(z - t >= 0)
         def _():
-            p = (z - t) * G + x
-            wait_slab(g, p)
-            forward(g, p, True, False)
+            wcopy(g, z - t, 0).wait_recv()
+            forward(g, z - t, True, False)
 
         @pl.when(z + t < Z)
         def _():
-            p = (z + t) * G + x
-            wait_slab(g, p)
-            forward(g, p, False, True)
+            wcopy(g, z + t, 0).wait_recv()
+            forward(g, z + t, False, True)
 
     def relays(g, low, high):
         def one(t, _):
@@ -144,38 +146,21 @@
             return 0
         lax.fori_loop(low, high, one, 0)
 
-    def finish(g):
-        if G > 1:
-            def one(zz, _):
-                wait_slab(g, zz * G + lax.rem(x + 1, G))
-                return 0
-            lax.fori_loop(0, Z, one, 0)
-
     def drain(g):
         def one(zz, _):
-            p = zz * G + x
-
             @pl.when((zz <= z) & (z + 1 < Z))
             def _():
-                wcopy(g, p, 0).wait_send()
+                wcopy(g, zz, 0).wait_send()
 
             @pl.when((zz >= z) & (z > 0))
             def _():
-                wcopy(g, p, 1).wait_send()
-
-            if G > 1:
-                wcopy(g, p, 2).wait_send()
+                wcopy(g, zz, 1).wait_send()
             return 0
         lax.fori_loop(0, Z, one, 0)
 
     for i in range(4):
         locals_[i].wait()
-    forward(0, me, True, True)
-    locals_[4].wait()
-    forward(1, me, True, True)
-    for i in (5, 6):
-        locals_[i].wait()
-    forward(2, me, True, True)
+    forward(0, z, True, True)
 
     half = E // 2
     lane = iota((R, E), 1)
@@ -199,17 +184,44 @@
         u = tokbuf[t].astype(f32)
         total = total + jnp.sum(u * u, axis=1, keepdims=True)
     inverse = lax.rsqrt(total / (T * F) + epsilon)
-    for t in range(T):
-        normed[:, t * F:(t + 1) * F] = (
-            tokbuf[t].astype(f32) * inverse * gain_ref[:, t * F:(t + 1) * F]).astype(bf16)
-    pre_w = jnp.dot(normed[...], ww_ref[...], preferred_element_type=f32)
-    pre_d = jnp.dot(normed[...], wd_ref[...], preferred_element_type=f32)
+    pre_w = jnp.zeros((R, ww_ref.shape[0]), f32)
+    pre_d = jnp.zeros((R, wd_ref.shape[0]), f32)
+    wide = rows if G > 1 else F
+    for g in range(G):
+        c = lax.rem(x + g + 1, G) if G > 1 else 0
+        for t in range(T * F // (wide * G)):
+            at = t * wide * G + c * wide
+            inner = pl.ds(pl.multiple_of(at % F, 128) if G > 1 else at % F, wide)
+            cols = pl.ds(pl.multiple_of(at, 128) if G > 1 else at, wide)
+            tok = tokbuf[t * wide * G // F, :, inner].astype(f32)
+            piece = (tok * inverse * gain_ref[:, cols]).astype(bf16)
+            pre_w = pre_w + dot_nt(piece, ww_ref[:, cols], None)
+            pre_d = pre_d + dot_nt(piece, wd_ref[:, cols], None)
+            if g + 1 == G:
+                feats[x, :, t * wide:(t + 1) * wide] = piece
+            else:
+                away[:, t * wide:(t + 1) * wide] = piece
+        if g + 1 < G:
+            pair_copy(0, away, feats.at[x]).start()
     all_heads = pre_w.shape[1]
     head_lane = iota((R, all_heads), 1)
 
     relays(0, 1, Z)
-    finish(0)
-    proj = jnp.dot(normed[...], Wd[...], preferred_element_type=f32)
+    locals_[4].wait()
+    forward(1, z, True, True)
+
+    def project(i, weight, mine_out, landing):
+        if G == 1:
+            return jnp.dot(feats[0], weight[...], preferred_element_type=f32)
+        mine_out[...] = jnp.dot(feats[other], weight[...], preferred_element_type=f32)
+        pair_copy(i, mine_out, landing).start()
+        half_sum = jnp.dot(feats[x], weight[...], preferred_element_type=f32)
+        pair_copy(i, mine_out, landing).wait_recv()
+        return half_sum + landing[...]
+
+    if G > 1:
+        pair_copy(0, away, feats.at[other]).wait_recv()
+    proj = project(1, Wd, dpart, dpart_in)
 
     ri = iota((R, R), 0)
     rj = iota((R, R), 1)
@@ -223,6 +235,9 @@
         size *= 2
     keep = []
     for h in range(H):
+        if h > 0 and Z > 2:
+            relay(1, h)
+
         def head(n):
             return proj[:, n * dc + h * E:n * dc + (h + 1) * E]
         q = unit_rows(silu(head(0))) * E ** (-0.5)
@@ -233,8 +248,8 @@
         decay = jnp.sum(jnp.where(chosen, pre_d, 0.0), axis=1, keepdims=True)
         beta = 1.0 / (1.0 + jnp.exp(-write))
         soft = jnp.maximum(decay, 0.0) + jnp.log1p(jnp.exp(-jnp.abs(decay)))
-        logd = offs_ref[:, h:h + 1] - scale_ref[h] * soft
-        C = dot_nn(tril, jnp.broadcast_to(logd, (R, R)))
+        logd = jnp.broadcast_to(offs_ref[h:h + 1, :], (R, R)).T - scale_ref[h] * soft
+        C = dot_nn(tril, logd)
         Dm = jnp.where(lower, jnp.exp(jnp.where(lower, C - C.T, 0.0)), 0.0)
         N = dot_nt(k * beta, k) * Dm
         X = jnp.where(ri == rj, 1.0, 0.0) - jnp.where(levels[0], N, 0.0)
@@ -256,14 +271,15 @@
             src_ref=st.at[p], dst_ref=st.at[p], send_sem=st_send.at[d], recv_sem=st_recv.at[p],
             device_id={"sp": lax.rem(me + d, S)}, device_id_type=MESH)
 
-    relays(1, 1, Z)
-
     def st_start(d, _):
         st_copy(d, me).start()
         return 0
+    relays(1, H if Z > 2 else 1, Z)
     lax.fori_loop(1, S - me, st_start, 0)
-    finish(1)
-    wproj = jnp.dot(normed[...], Ww[...], preferred_element_type=f32)
+    for i in (5, 6):
+        locals_[i].wait()
+    forward(2, z, True, True)
+    wproj = project(2, Ww, wpart, wpart_in)
 
     def rope(u):
         return u * cosine + dot_nn(u, swap) * sine
@@ -278,7 +294,8 @@
             src_ref=edge_own, dst_ref=edge_in, send_sem=edge_send, recv_sem=edge_recv,
             device_id={"sp": lax.rem(me + 1, S)}, device_id_type=MESH)
     edge_copy().start()
-    relays(2, 1, Z)
+    if Z > 1:
+        relay(2, 1)
     edge_copy().wait_recv()
     k_prev = edge_in[:, 0:kc]
     v_prev = edge_in[:, kc:2 * kc]
@@ -293,10 +310,13 @@
         row_total = (jnp.sum(e_cur, axis=1, keepdims=True) + jnp.sum(e_prev, axis=1, keepdims=True)
                      + jnp.exp(sink - top))
         logt_ref[:, h:h + 1] = top + jnp.log(row_total)
+        if h == 1 and Z > 2:
+            relay(2, 2)
         mixed_rows = (dot_nn((e_cur / row_total).astype(bf16), v_cur, None)
                       + dot_nn((e_prev / row_total).astype(bf16), v_prev, None))
-        mix[:, dc + h * E:dc + (h + 1) * E] = mixed_rows.astype(bf16)
-
+        mix[x, :, dc + h * E:dc + (h + 1) * E] = mixed_rows.astype(bf16)
+
+    relays(2, min(3 if QH > 1 else 2, Z), Z)
     def chain(p, carry):
         pltpu.make_async_remote_copy(
             src_ref=st.at[p], dst_ref=st.at[p], send_sem=st_send.at[0], recv_sem=st_recv.at[p],
@@ -310,27 +330,52 @@
         o = keep[h][0] + dot_nn(keep[h][1], memory[h])
         o = o * lax.rsqrt(jnp.mean(o * o, axis=1, keepdims=True) + epsilon) * ngain_ref[...]
         gate = proj[:, 3 * dc + h * E:3 * dc + (h + 1) * E]
-        mix[:, h * E:(h + 1) * E] = (o * silu(gate)).astype(bf16)
-
-    finish(2)
-    part[...] = dot_nt(mix[...], Wo[...], None).astype(bf16)
+        mix[x, :, h * E:(h + 1) * E] = (o * silu(gate)).astype(bf16)
+
+    if G > 1:
+        pair_copy(3, mix.at[x], mix.at[x]).start()
+        part[x] = dot_nt(mix[x], Wo[...], None).astype(bf16)
+        pair_copy(3, mix.at[x], mix.at[other]).wait_recv()
+        part[other] = dot_nt(mix[other], Wo[...], None).astype(bf16)
+    else:
+        part[0] = dot_nt(mix[0], Wo[...], None).astype(bf16)
     r = R // T
 
     def out_copy(d, source):
         peer = lax.rem(j + d, T)
         return pltpu.make_async_remote_copy(
-            src_ref=part.at[pl.ds(pl.multiple_of(peer * r, r), r), :], dst_ref=partin.at[source],
+            src_ref=part.at[:, pl.ds(pl.multiple_of(peer * r, r), r), :], dst_ref=partin.at[source],
             send_sem=out_send.at[d], recv_sem=out_recv.at[source],
             device_id={"tp": peer}, device_id_type=MESH)
     for d in range(1, T):
         out_copy(d, j).start()
-    partin[j] = part[pl.ds(pl.multiple_of(j * r, r), r), :]
+    partin[j] = part[:, pl.ds(pl.multiple_of(j * r, r), r), :]
     for d in range(1, T):
         out_copy(d, lax.rem(j + d, T)).wait_recv()
-    acc = partin[0].astype(f32)
-    for t in range(1, T):
-        acc = acc + partin[t].astype(f32)
-    mixed_ref[...] = acc.astype(bf16)
+
+    def reduced(slot):
+        acc = partin[0, slot].astype(f32)
+        for t in range(1, T):
+            acc = acc + partin[t, slot].astype(f32)
+        return acc.astype(bf16)
+    if G > 1:
+        red[...] = reduced(other)
+        pair_copy(4, red, red_in).start()
+        done = reduced(x)
+        for zz in range(Z):
+            at = pl.multiple_of(zz * G * rows + x * rows, 128)
+            mixed_ref[:, pl.ds(at, rows)] = done[:, zz * rows:(zz + 1) * rows]
+        pair_copy(4, red, red_in).wait_recv()
+        for zz in range(Z):
+            at = pl.multiple_of(zz * G * rows + other * rows, 128)
+            mixed_ref[:, pl.ds(at, rows)] = red_in[:, zz * rows:(zz + 1) * rows]
+        pair_copy(0, away, feats.at[x]).wait_send()
+        pair_copy(1, dpart, dpart_in).wait_send()
+        pair_copy(2, wpart, wpart_in).wait_send()
+        pair_copy(3, mix.at[x], mix.at[x]).wait_send()
+        pair_copy(4, red, red_in).wait_send()
+    else:
+        mixed_ref[...] = reduced(0)
 
     for d in range(1, T):
         out_copy(d, j).wait_send()
@@ -348,40 +393,51 @@
 def shards(S, T, tokens, gain, dq, dk, dv, dz, ww, wd, bias, scale, offs, ngain, do, wq, wk, wv, sink, wo):
     R, F = tokens.shape
     D = F * T
+    rows = dq.shape[0]
     dc = dq.shape[1]
     H = bias.shape[0]
     E = dc // H
     qc, kc = wq.shape[1], wk.shape[1]
-    G = 2 if S % 2 == 0 else 1
+    G = 2 if S % 2 == 0 and rows % 128 == 0 and F % (2 * rows) == 0 else 1
     Z = S // G
+    K = D // G
     vmem = pl.BlockSpec(memory_space=pltpu.VMEM)
     smem = pl.BlockSpec(memory_space=pltpu.SMEM)
     hbm = pl.BlockSpec(memory_space=pl.ANY)
     dma = pltpu.SemaphoreType.DMA
+    V = pltpu.VMEM
     return pl.pallas_call(
         functools.partial(layer_kernel, S, T, G),
         out_shape=(jax.ShapeDtypeStruct((R // T, D), bf16), jax.ShapeDtypeStruct((R, sink.shape[0]), f32)),
         in_specs=[vmem, vmem, hbm, hbm, hbm, hbm, vmem, vmem, smem, smem, vmem, vmem, hbm, hbm, vmem, vmem, smem, hbm],
         out_specs=(vmem, vmem),
         scratch_shapes=[
-            pltpu.VMEM((T, R, F), bf16),
-            pltpu.VMEM((R, D), bf16),
-            pltpu.VMEM((D, 4 * dc), bf16),
-            pltpu.VMEM((D, qc + 2 * kc), bf16),
-            pltpu.VMEM((D, dc + qc), bf16),
-            pltpu.VMEM((S, H, E, 2 * E), f32),
-            pltpu.VMEM((R, 2 * kc), bf16),
-            pltpu.VMEM((R, 2 * kc), bf16),
-            pltpu.VMEM((R, dc + qc), bf16),
-            pltpu.VMEM((R, D), bf16),
-            pltpu.VMEM((T, R // T, D), bf16),
-            pltpu.VMEM((H, E, E), f32),
-            dma((8,)), dma((T,)), dma((T,)), dma((3, 3, Z)), dma((3, S)), dma((S,)), dma((S,)),
-            dma, dma, dma((T,)), dma((T,)),
+            V((T, R, F), bf16),
+            V((G, R, K), bf16),
+            V((R, K), bf16),
+            V((K, 4 * dc), bf16),
+            V((K, qc + 2 * kc), bf16),
+            V((K, dc + qc), bf16),
+            V((R, 4 * dc), f32),
+            V((R, 4 * dc), f32),
+            V((R, qc + 2 * kc), f32),
+            V((R, qc + 2 * kc), f32),
+            V((S, H, E, 2 * E), f32),
+            V((R, 2 * kc), bf16),
+            V((R, 2 * kc), bf16),
+            V((G, R, dc + qc), bf16),
+            V((G, R, K), bf16),
+            V((T, G, R // T, K), bf16),
+            V((R // T, K), bf16),
+            V((R // T, K), bf16),
+            V((H, E, E), f32),
+            dma((8,)), dma((T,)), dma((T,)), dma((3, 2, Z)), dma((3, Z)), dma((S,)), dma((S,)),
+            dma, dma, dma((T,)), dma((T,)), dma((5,)), dma((5,)),
         ],
         compiler_params=pltpu.CompilerParams(
             collective_id=0, has_side_effects=True, vmem_limit_bytes=60 * 1024 * 1024),
-    )(tokens, gain.reshape(1, D), dq, dk, dv, dz, ww, wd, bias, scale, offs, ngain.reshape(1, E), do, wq, wk, wv, sink, wo)
+    )(tokens, gain.reshape(1, D), dq, dk, dv, dz, ww.T, wd.T, bias, scale, offs.T, ngain.reshape(1, E), do, wq, wk.T,
+      wv.T, sink, wo)
 
 
 def solution(mesh):

time: 96.5 us -> 83 us (0.86); the launches traced: 96.1 us -> 81.5 us
  Pallas kernels: 87.5 us -> 77.8 us
  local copies, waits for them, and re-layouts: 8 us -> 3.06 us
    pallas_call x1, Pallas kernels: 87.5 us -> 77.8 us  [shards(): pl.pallas_call(functools.partial(layer_kernel, S, T, G), out_shape=(jax.S...]
    unnamed x16 -> x1, local copies, waits for them, and re-layouts: 6.51 us -> 1.57 us
where the time goes in v2:
time: 83 us; the launch traced here: 81.5 us
  Pallas kernels  77.8 us (94%)
  local copies, waits for them, and re-layouts  3.06 us (4%)
    pallas_call x1, Pallas kernels, shards(): pl.pallas_call(functools.partial(layer_kernel, S, T, G), out_shape=(jax.S...  77.8 us

profile of v2, /device:TPU:25, one launch (start us, length us, event | category | flops | bytes accessed | tf_op | source)
XLA Modules:
  0.0 81.5 jit_solution(16062167980496701695)
XLA Ops:
  0.6 77.8 %shard_map.185 = (bf16[32,2048]{1,0:T(8,128)(2,1)}, f32[128,4]{1,0:T(8,128)}) custom-call(bf16[128,512]{1,0:T(8,128)(2,1)} %tok_ref.1, f32[1,2048]{1,0:T(1,128)} %bitcast.11, bf16[256,128]{1,0:T(8,128)(2,1)} %dq_ref.1, bf16[256,128]{1,0:T(8,128)(2,1)} %dk_ref.1, bf16[256,128]{1,0:T(8,128)(2,1)} %dv_ref.1, bf16[256,128]{1,0:T(8,128)(2,1)} %dz_ref.1, ...), custom_call_target="tpu_custom_call" | custom-call | tf_op jit(solution)/shard_map/pallas_call | solution.py:409
  78.5 1.5 %copy.20 = f32[128,4]{0,1:T(4,128)} copy(f32[128,4]{1,0:T(8,128)} %get-tuple-element.3) | data formatting | bytes 4096 | tf_op jit(solution)/shard_map/pallas_call | solution.py:409
  80.0 1.6 %copy.22 = bf16[32,2048]{1,0:T(8,128)(2,1)} copy(bf16[32,2048]{1,0:T(8,128)(2,1)} %get-tuple-element.6) | data formatting | bytes 262144
